TPU v7x, 32 devices: a whole 2x2x4 slice. The times are simulated.
32 devices in a mesh: grp: 2 (over y), sp: 4 (over z), dp: 4 (over x, core).
Axes of the slice: x: 2, y: 2, z: 4, core: 2. Of those that a mesh axis runs over, the one named last changes fastest.
Arguments:
- activations: bfloat16 [8, 2048, 2048], P(('grp', 'dp'), 'sp'), parts along dimension 0, may hold values from -6 to 6
- value_weight: bfloat16 [2048, 1024], P('sp', 'dp'), may hold values from -0.125 to 0.125
- gate_weight: bfloat16 [2048, 1024], P('sp', 'dp'), may hold values from -0.125 to 0.125
- conv_taps: float32 [31, 1024], replicated, may hold values from -4 to 4
- conv_bias: float32 [1024], replicated, may hold values from -3 to 3
- norm_gain: float32 [1024], replicated, may hold values from 0.1 to 1.9
- norm_bias: float32 [1024], replicated, may hold values from -3 to 3
- out_weight: bfloat16 [1024, 2048], P('sp', 'dp'), may hold values from -0.1875 to 0.1875
Outputs:
- mixed_out: bfloat16 [8, 2048, 2048], P(('grp', 'dp'), 'sp'), parts along dimension 0
There are 2 independent parts, one for each index of `grp`. A program takes and returns all parts, laid end to end along the dimension named above; an argument that names none is the same for every part. Nothing has to cross between parts.
All inputs are finite; a program needn't handle non-finite values.
Results may differ from a plain program's by a relative error of at most 0.013.
Values may be sent and summed in bfloat16 or wider, within the bound.
A program may use at most 64 MiB of HBM per device.

v0:
```python
import jax
import jax.numpy as jnp
from jax import lax
from jax.sharding import PartitionSpec as P

epsilon = 1e-05


def passed_along(value, axis, steps):
    count = lax.axis_size(axis)
    first, last = (max(0, -steps), min(count, count - steps))
    return lax.ppermute(value, axis, [(source, source + steps) for source in range(first, last)])


def local(
    activations, value_weight, gate_weight, conv_taps, conv_bias, norm_gain, norm_bias, out_weight
):
    tokens = activations[0]
    tok_rows = tokens.shape[0]
    kernel_len = conv_taps.shape[0]
    whole_value, whole_gate = (
        lax.all_gather(value_weight, "sp", axis=0, tiled=True),
        lax.all_gather(gate_weight, "sp", axis=0, tiled=True),
    )
    stacked = jnp.stack([whole_value, whole_gate], axis=0)
    both_rows = jnp.einsum(
        "td,kdc->ktc",
        tokens,
        lax.all_gather(stacked, "dp", axis=2, tiled=True),
        preferred_element_type=jnp.float32,
    )
    value_rows = both_rows[0]
    gate_rows = both_rows[1]
    value_half = value_rows.astype(jnp.bfloat16)
    gate_half = gate_rows.astype(jnp.bfloat16)
    gated_rows = (
        value_half.astype(jnp.float32) * jax.nn.sigmoid(gate_half.astype(jnp.float32))
    ).astype(jnp.bfloat16)
    prior = passed_along(gated_rows[tok_rows - (kernel_len - 1) :], "sp", 1)
    padded = jnp.concatenate([prior, gated_rows], axis=0).astype(jnp.float32)
    conv_sum = jnp.zeros(gated_rows.shape, jnp.float32) + conv_bias[None, :]
    for tap_index in range(kernel_len):
        conv_sum = (
            conv_sum + conv_taps[tap_index][None, :] * padded[tap_index : tap_index + tok_rows]
        )
    mean_row = jnp.mean(conv_sum, axis=-1, keepdims=True)
    centered = conv_sum - mean_row
    spread = jnp.mean(centered * centered, axis=-1, keepdims=True)
    normed = centered * lax.rsqrt(spread + epsilon) * norm_gain[None, :] + norm_bias[None, :]
    swished = jax.nn.silu(normed).astype(jnp.bfloat16)
    whole_output = lax.all_gather(out_weight, "sp", axis=0, tiled=True)
    result = jnp.dot(
        swished,
        lax.all_gather(whole_output, "dp", axis=1, tiled=True),
        preferred_element_type=jnp.float32,
    )
    return result.astype(jnp.bfloat16)[None]


def solution(mesh):
    in_specs = (
        P(("grp", "dp"), "sp", None),
        P("sp", "dp"),
        P("sp", "dp"),
        P(),
        P(),
        P(),
        P(),
        P("sp", "dp"),
    )
    out_specs = P(("grp", "dp"), "sp", None)
    return jax.shard_map(local, mesh=mesh, in_specs=in_specs, out_specs=out_specs, check_vma=False)
```

profile of v0, /device:TPU:0, one launch (start us, length us, event | category | flops | bytes accessed | tf_op | source)
XLA Modules:
  0.0 207.2 jit_solution(12494679978274099827)
XLA Ops:
  6.5 0.7 all-gather.6.cloned.1.call-update
  7.3 0.0 all-gather.8.cloned.1.call-start
  7.3 0.7 all-gather.8.cloned.1.call-update
  8.0 0.0 all-gather.12.cloned.1.call-start
  8.1 0.7 all-gather.12.cloned.1.call-update
  8.7 0.0 all-gather.10.cloned.1.call-start
  8.8 30.9 %all-gather.6.cloned.1.call-done = bf16[2048,256]{1,0:T(8,128)(2,1)} async-done(((bf16[512,256]{1,0:T(8,128)(2,1)}), bf16[2048,256]{1,0:T(8,128)(2,1)}) %all-gather.6.cloned.1.call-update) | async-done | bytes 1048592 | tf_op jit(solution)/shard_map/all_gather | solution.py:22
  39.6 29.0 %all-gather.8.cloned.1.call-done = bf16[2048,256]{1,0:T(8,128)(2,1)} async-done(((bf16[512,256]{1,0:T(8,128)(2,1)}), bf16[2048,256]{1,0:T(8,128)(2,1)}) %all-gather.8.cloned.1.call-update) | async-done | bytes 1048592 | tf_op jit(solution)/shard_map/all_gather | solution.py:23
  68.6 3.1 %pad_maximum_fusion = bf16[2,2048,256]{2,1,0:T(8,128)(2,1)} fusion(bf16[1,2048,256]{2,1,0:T(8,128)(2,1)} %bitcast.50, bf16[1,2048,256]{2,1,0:T(8,128)(2,1)} %bitcast.49), kind=kLoop, calls=%fused_computation.64 | loop fusion | flops 1048576 | bytes 4194304 | tf_op jit(solution)/shard_map/stack | solution.py:25
  71.7 0.0 all-gather.10.cloned.1.call-update
  71.7 0.0 all-gather.14.cloned.1.call-start
  71.7 25.8 %all-gather.12.cloned.1.call-done = bf16[1024,512]{1,0:T(8,128)(2,1)} async-done(((bf16[256,512]{1,0:T(8,128)(2,1)}), bf16[1024,512]{1,0:T(8,128)(2,1)}) %all-gather.12.cloned.1.call-update) | async-done | bytes 1048592 | tf_op jit(solution)/shard_map/all_gather | solution.py:51
  97.6 0.0 all-gather.14.cloned.1.call-update
  97.6 0.0 copy-done.2
  97.6 0.1 fusion.44
  97.7 60.0 %all-gather.10.cloned.1.call-done = bf16[2,2048,1024]{2,1,0:T(8,128)(2,1)} async-done(((bf16[2,2048,256]{2,1,0:T(8,128)(2,1)}), bf16[2,2048,1024]{2,1,0:T(8,128)(2,1)}) %all-gather.10.cloned.1.call-update) | async-done | bytes 8388624 | tf_op jit(solution)/shard_map/all_gather | solution.py:29
  157.8 0.0 copy-done
  157.8 8.1 %convert_bitcast_fusion = bf16[2,512,1024]{2,1,0:T(8,128)(2,1)S(1)} fusion(bf16[2,2048,1024]{2,1,0:T(8,128)(2,1)} %all-gather.10.cloned.1.call-done, bf16[1,512,2048]{2,1,0:T(8,128)(2,1)S(1)} %copy-done), kind=kOutput, calls=%fused_computation.68 | convolution fusion | flops 4296015872 | bytes 12582912 | tf_op jit(solution)/shard_map/td,kdc->ktc/dot_general | solution.py:26
  165.8 0.6 multiply_convert_fusion
  166.5 3.4 %collective-permute-start = (bf16[30,1024]{1,0:T(8,128)(2,1)S(1)}, bf16[30,1024]{1,0:T(8,128)(2,1)S(1)}, u32[]{:S(2)}, u32[]{:S(2)}) collective-permute-start(bf16[30,1024]{1,0:T(8,128)(2,1)S(1)} %slice_bitcast_fusion), channel_id=1, source_target_pairs={{0,4},{4,8},{8,12},{1,5},{5,9},{9,13},{2,6},{6,10},{10,14},{3,7},{... | collective-permute-start | bytes 184328 | tf_op jit(solution)/shard_map/ppermute | solution.py:12
  169.9 0.6 fusion.48
  170.5 0.0 copy-start.3
  170.5 1.3 collective-permute-done
  171.8 0.3 maximum_convert_fusion
  172.1 9.8 %fusion.42 = (f32[512]{0:T(512)S(1)}, f32[512,1024]{1,0:T(8,128)S(1)}) fusion(f32[542,1024]{1,0:T(8,128)S(1)} %maximum_convert_fusion, f32[1024]{0:T(1024)S(1)} %bitcast.61, f32[1024]{0:T(1024)S(1)} %bitcast.62, f32[1024]{0:T(1024)S(1)} %bitcast.64, f32[1024]{0:T(1024)S(1)} %bitcast.65, f32[1024]{0:T(1024)S(1)} %bitcast.66, f32[1024]{0:T(1024)S(1)} %bitcast.67, ...), kind=kLoop, calls=%fused_computation.81 | loop fusion | flops 33029632 | bytes 67241984 | tf_op jit(solution)/shard_map/reduce_sum | solution.py:46
  181.9 0.0 copy-start.4
  181.9 0.0 copy-start.5
  182.0 1.3 copy-done.1
  183.3 0.3 multiply_reduce_fusion
  183.6 10.0 %all-gather.14.cloned.1.call-done = bf16[1024,2048]{1,0:T(8,128)(2,1)} async-done(((bf16[1024,512]{1,0:T(8,128)(2,1)}), bf16[1024,2048]{1,0:T(8,128)(2,1)}) %all-gather.14.cloned.1.call-update) | async-done | bytes 4194320 | tf_op jit(solution)/shard_map/all_gather | solution.py:54
  193.7 0.0 copy-done.5
  193.7 7.0 %fusion = bf16[1,512,2048]{2,1,0:T(8,128)(2,1)} fusion(bf16[1024,2048]{1,0:T(8,128)(2,1)} %all-gather.14.cloned.1.call-done, f32[512,1024]{1,0:T(8,128)} %copy-done.1, f32[1024]{0:T(1024)S(1)} %copy-done.4, f32[1024]{0:T(1024)S(1)} %copy-done.5, f32[512]{0:T(512)S(1)} %add_rsqrt_fusion, f32[512]{0:T(512)S(1)} %broadcast_multiply_fusion), kind=kOutput, calls=%fused_computation.1 | convolution fusion | flops 2153250816 | bytes 8400896 | tf_op jit(solution)/shard_map/dot_general | solution.py:52
  (10 shorter events, 0.1 us)
Async XLA Ops:
  6.5 151.2 %copy-start = (bf16[1,512,2048]{2,1,0:T(8,128)(2,1)S(1)}, bf16[1,512,2048]{2,1,0:T(8,128)(2,1)}, u32[]{:S(2)}) copy-start(bf16[1,512,2048]{2,1,0:T(8,128)(2,1)} %param.8) | copy-start | bytes 6291460
  6.5 33.1 %all-gather.6.cloned.1.call-start = ((), (), s32[]{:S(2)}) async-start(), calls=%async_computation | async-start | bytes 1310720 | tf_op jit(solution)/shard_map/all_gather | solution.py:22
  7.3 61.3 %all-gather.8.cloned.1.call-start = ((), (), s32[]{:S(2)}) async-start(), calls=%async_computation.1 | async-start | bytes 1310720 | tf_op jit(solution)/shard_map/all_gather | solution.py:23
  8.0 89.6 %all-gather.12.cloned.1.call-start = ((), (), s32[]{:S(2)}) async-start(), calls=%async_computation.3 | async-start | bytes 1310720 | tf_op jit(solution)/shard_map/all_gather | solution.py:51
  8.7 149.0 %all-gather.10.cloned.1.call-start = ((), (), s32[]{:S(2)}) async-start(), calls=%async_computation.2 | async-start | bytes 10485760 | tf_op jit(solution)/shard_map/all_gather | solution.py:29
  71.7 25.9 %copy-start.2 = (f32[31,1024]{1,0:T(8,128)S(1)}, f32[31,1024]{1,0:T(8,128)}, u32[]{:S(2)}) copy-start(f32[31,1024]{1,0:T(8,128)} %param.11) | copy-start | bytes 380932
  71.7 122.0 %all-gather.14.cloned.1.call-start = ((), (), s32[]{:S(2)}) async-start(), calls=%async_computation.4 | async-start | bytes 5242880 | tf_op jit(solution)/shard_map/all_gather | solution.py:54
  166.5 5.3 %collective-permute-start = (bf16[30,1024]{1,0:T(8,128)(2,1)S(1)}, bf16[30,1024]{1,0:T(8,128)(2,1)S(1)}, u32[]{:S(2)}, u32[]{:S(2)}) collective-permute-start(bf16[30,1024]{1,0:T(8,128)(2,1)S(1)} %slice_bitcast_fusion), channel_id=1, source_target_pairs={{0,4},{4,8},{8,12},{1,5},{5,9},{9,13},{2,6},{6,10},{10,14},{3,7},{... | collective-permute-start | bytes 184328 | tf_op jit(solution)/shard_map/ppermute | solution.py:12
  170.5 1.6 copy-start.3
  181.9 1.3 copy-start.1
  181.9 11.7 %copy-start.4 = (f32[1024]{0:T(1024)S(1)}, f32[1024]{0:T(1024)}, u32[]{:S(2)}) copy-start(f32[1024]{0:T(1024)} %param.14) | copy-start | bytes 12292
  181.9 11.7 %copy-start.5 = (f32[1024]{0:T(1024)S(1)}, f32[1024]{0:T(1024)}, u32[]{:S(2)}) copy-start(f32[1024]{0:T(1024)} %param.13) | copy-start | bytes 12292
Sparse Core Ops, SparseCore 0:
  8.9 30.6 all-gather.5
  41.2 27.3 all-gather.7
  70.2 27.3 all-gather.11
  99.0 58.7 all-gather.9
  159.2 34.4 all-gather.13
where the time goes:
time: 207 us
  waiting for transfers between devices  159 us (77%)
  matrix products  15 us (7%)
  other arithmetic  14.7 us (7%)
  between operations  13.3 us (6%)
  starting transfers between devices  3.55 us (2%)
    all_gather x1, waiting for transfers between devices, local(): lax.all_gather(stacked, 'dp', axis=2, tiled=True)  60 us
    all_gather x1, waiting for transfers between devices, local(): lax.all_gather(value_weight, 'sp', axis=0, tiled=True)  30.9 us
    all_gather x1, waiting for transfers between devices, local(): lax.all_gather(gate_weight, 'sp', axis=0, tiled=True)  29 us
    all_gather x1, waiting for transfers between devices, local(): whole_output = lax.all_gather(out_weight, 'sp', axis=0, tiled=True)  25.8 us
    all_gather x1, waiting for transfers between devices, local(): lax.all_gather(whole_output, 'dp', axis=1, tiled=True)  10 us
    reduce_sum x1, other arithmetic, local(): mean_row = jnp.mean(conv_sum, axis=-1, keepdims=True)  9.83 us
    dot_general x1, matrix products, local(): jnp.einsum('td,kdc->ktc', tokens, lax.all_gather(stacked, 'dp', axis=2, t...  8.06 us
    dot_general x1, matrix products, local(): jnp.dot(swished, lax.all_gather(whole_output, 'dp', axis=1, tiled=True),...  6.96 us
  transfers between devices with their start and end apart: 6, of which 6 were waited for; matrix products, arithmetic and copies ran while one was open for 11% of the time, Pallas kernels for 0%

commit v1 on v0

--- a/solution.py
+++ b/solution.py
@@ -4,6 +4,17 @@
 from jax.sharding import PartitionSpec as P
 
 epsilon = 1e-05
+
+
+def pass_along(x, axis, dim):
+    size = lax.axis_size(axis)
+    right = [(i, (i + 1) % size) for i in range(size)]
+    parts = [x]
+    for hop in range(1, size):
+        parts = [lax.ppermute(parts[0], axis, right), *parts]
+    whole = jnp.concatenate(parts, axis=dim)
+    turn = (lax.axis_index(axis) + 1) * parts[-1].shape[dim]
+    return jnp.roll(whole, turn, axis=dim)
 
 
 def passed_along(value, axis, steps):
@@ -48,7 +59,7 @@
     spread = jnp.mean(centered * centered, axis=-1, keepdims=True)
     normed = centered * lax.rsqrt(spread + epsilon) * norm_gain[None, :] + norm_bias[None, :]
     swished = jax.nn.silu(normed).astype(jnp.bfloat16)
-    whole_output = lax.all_gather(out_weight, "sp", axis=0, tiled=True)
+    whole_output = pass_along(out_weight, "sp", 0)
     result = jnp.dot(
         swished,
         lax.all_gather(whole_output, "dp", axis=1, tiled=True),

time: 207 us -> 180 us (0.87)
  waiting for transfers between devices: 159 us -> 128 us
  local copies, waits for them, and re-layouts: 1.44 us -> 3.57 us
    all_gather x1, waiting for transfers between devices: 60 us -> 30.5 us  [local(): lax.all_gather(stacked, 'dp', axis=2, tiled=True)]
    all_gather x1 -> x0, waiting for transfers between devices: 25.8 us -> none  [local(): whole_output = lax.all_gather(out_weight, 'sp', axis=0, tiled=True)]
    ppermute x0 -> x3, waiting for transfers between devices: none -> 24.6 us  [pass_along(): parts = [lax.ppermute(parts[0], axis, right), *parts]]
  transfers between devices with their start and end apart: 6 -> 8, of which waited for: 6 -> 8; matrix products, arithmetic and copies ran while one was open for 11% -> 12% of each run, Pallas kernels for 0% -> 0%
where the time goes in v1:
time: 180 us
  waiting for transfers between devices  128 us (71%)
  matrix products  15 us (8%)
  other arithmetic  14.7 us (8%)
  between operations  13.3 us (7%)
  starting transfers between devices  4.97 us (3%)
  local copies, waits for them, and re-layouts  3.57 us (2%)
    all_gather x1, waiting for transfers between devices, local(): lax.all_gather(value_weight, 'sp', axis=0, tiled=True)  31.6 us
    all_gather x1, waiting for transfers between devices, local(): lax.all_gather(stacked, 'dp', axis=2, tiled=True)  30.5 us
    all_gather x1, waiting for transfers between devices, local(): lax.all_gather(gate_weight, 'sp', axis=0, tiled=True)  29 us
    ppermute x3, waiting for transfers between devices, pass_along(): parts = [lax.ppermute(parts[0], axis, right), *parts]  24.6 us
    all_gather x1, waiting for transfers between devices, local(): lax.all_gather(whole_output, 'dp', axis=1, tiled=True)  10.1 us
    reduce_sum x1, other arithmetic, local(): mean_row = jnp.mean(conv_sum, axis=-1, keepdims=True)  9.83 us
    dot_general x1, matrix products, local(): jnp.einsum('td,kdc->ktc', tokens, lax.all_gather(stacked, 'dp', axis=2, t...  8.07 us
    dot_general x1, matrix products, local(): jnp.dot(swished, lax.all_gather(whole_output, 'dp', axis=1, tiled=True),...  6.97 us
  transfers between devices with their start and end apart: 8, of which 8 were waited for; matrix products, arithmetic and copies ran while one was open for 12% of the time, Pallas kernels for 0%

profile of v1, /device:TPU:0, one launch (start us, length us, event | category | flops | bytes accessed | tf_op | source)
XLA Modules:
  0.0 180.0 jit_solution(5782916036457545505)
XLA Ops:
  6.5 0.7 all-gather.5.cloned.1.call-update
  7.3 0.0 all-gather.7.cloned.1.call-start
  7.3 0.7 all-gather.7.cloned.1.call-update
  8.0 0.0 all-gather.9.cloned.1.call-start
  8.1 31.6 %all-gather.5.cloned.1.call-done = bf16[2048,256]{1,0:T(8,128)(2,1)} async-done(((bf16[512,256]{1,0:T(8,128)(2,1)}), bf16[2048,256]{1,0:T(8,128)(2,1)}) %all-gather.5.cloned.1.call-update) | async-done | bytes 1048592 | tf_op jit(solution)/shard_map/all_gather | solution.py:33
  39.6 29.0 %all-gather.7.cloned.1.call-done = bf16[2048,256]{1,0:T(8,128)(2,1)} async-done(((bf16[512,256]{1,0:T(8,128)(2,1)}), bf16[2048,256]{1,0:T(8,128)(2,1)}) %all-gather.7.cloned.1.call-update) | async-done | bytes 1048592 | tf_op jit(solution)/shard_map/all_gather | solution.py:34
  68.6 3.1 %pad_maximum_fusion = bf16[2,2048,256]{2,1,0:T(8,128)(2,1)} fusion(bf16[1,2048,256]{2,1,0:T(8,128)(2,1)} %bitcast.50, bf16[1,2048,256]{2,1,0:T(8,128)(2,1)} %bitcast.49), kind=kLoop, calls=%fused_computation.64 | loop fusion | flops 1048576 | bytes 4194304 | tf_op jit(solution)/shard_map/stack | solution.py:36
  71.7 0.0 all-gather.9.cloned.1.call-update
  71.7 0.0 all-gather.11.cloned.1.call-start
  71.7 0.9 copy-done.2
  72.6 1.4 collective-permute-start.1
  74.1 7.9 %collective-permute-done.1 = bf16[256,512]{1,0:T(8,128)(2,1)S(1)} collective-permute-done((bf16[256,512]{1,0:T(8,128)(2,1)S(1)}, bf16[256,512]{1,0:T(8,128)(2,1)S(1)}, u32[]{:S(2)}, u32[]{:S(2)}) %collective-permute-start.1) | collective-permute-done | bytes 262176 | tf_op jit(solution)/shard_map/ppermute | solution.py:14
  82.0 8.5 %collective-permute-done.2 = bf16[256,512]{1,0:T(8,128)(2,1)S(1)} collective-permute-done((bf16[256,512]{1,0:T(8,128)(2,1)S(1)}, bf16[256,512]{1,0:T(8,128)(2,1)S(1)}, u32[]{:S(2)}, u32[]{:S(2)}) %collective-permute-start.2) | collective-permute-done | bytes 262176 | tf_op jit(solution)/shard_map/ppermute | solution.py:14
  90.5 8.2 %collective-permute-done.3 = bf16[256,512]{1,0:T(8,128)(2,1)S(1)} collective-permute-done((bf16[256,512]{1,0:T(8,128)(2,1)S(1)}, bf16[256,512]{1,0:T(8,128)(2,1)S(1)}, u32[]{:S(2)}, u32[]{:S(2)}) %collective-permute-start.3) | collective-permute-done | bytes 262176 | tf_op jit(solution)/shard_map/ppermute | solution.py:14
  98.8 0.0 copy-start.3
  98.9 1.1 constant_dynamic-slice_fusion
  100.0 0.0 all-gather.11.cloned.1.call-update
  100.0 0.1 fusion.44
  100.1 30.5 %all-gather.9.cloned.1.call-done = bf16[2,2048,1024]{2,1,0:T(8,128)(2,1)} async-done(((bf16[2,2048,256]{2,1,0:T(8,128)(2,1)}), bf16[2,2048,1024]{2,1,0:T(8,128)(2,1)}) %all-gather.9.cloned.1.call-update) | async-done | bytes 8388624 | tf_op jit(solution)/shard_map/all_gather | solution.py:40
  130.6 8.1 %convert_bitcast_fusion = bf16[2,512,1024]{2,1,0:T(8,128)(2,1)S(1)} fusion(bf16[2,2048,1024]{2,1,0:T(8,128)(2,1)} %all-gather.9.cloned.1.call-done, bf16[1,512,2048]{2,1,0:T(8,128)(2,1)S(1)} %copy-done), kind=kOutput, calls=%fused_computation.68 | convolution fusion | flops 4296015872 | bytes 12582912 | tf_op jit(solution)/shard_map/td,kdc->ktc/dot_general | solution.py:37
  138.7 0.6 multiply_convert_fusion
  139.3 3.4 %collective-permute-start = (bf16[30,1024]{1,0:T(8,128)(2,1)S(1)}, bf16[30,1024]{1,0:T(8,128)(2,1)S(1)}, u32[]{:S(2)}, u32[]{:S(2)}) collective-permute-start(bf16[30,1024]{1,0:T(8,128)(2,1)S(1)} %slice_bitcast_fusion), channel_id=1, source_target_pairs={{0,4},{4,8},{8,12},{1,5},{5,9},{9,13},{2,6},{6,10},{10,14},{3,7},{... | collective-permute-start | bytes 184328 | tf_op jit(solution)/shard_map/ppermute | solution.py:23
  142.7 0.6 fusion.48
  143.3 1.3 collective-permute-done
  144.6 0.3 maximum_convert_fusion
  144.9 9.8 %fusion.42 = (f32[512]{0:T(512)S(1)}, f32[512,1024]{1,0:T(8,128)S(1)}) fusion(f32[542,1024]{1,0:T(8,128)S(1)} %maximum_convert_fusion, f32[1024]{0:T(1024)S(1)} %bitcast.61, f32[1024]{0:T(1024)S(1)} %bitcast.62, f32[1024]{0:T(1024)S(1)} %bitcast.64, f32[1024]{0:T(1024)S(1)} %bitcast.65, f32[1024]{0:T(1024)S(1)} %bitcast.66, f32[1024]{0:T(1024)S(1)} %bitcast.67, ...), kind=kLoop, calls=%fused_computation.90 | loop fusion | flops 33029632 | bytes 67241984 | tf_op jit(solution)/shard_map/reduce_sum | solution.py:57
  154.8 0.0 copy-start.5
  154.8 0.0 copy-start.6
  154.8 1.3 copy-done.1
  156.1 0.3 multiply_reduce_fusion
  156.4 10.1 %all-gather.11.cloned.1.call-done = bf16[1024,2048]{1,0:T(8,128)(2,1)} async-done(((bf16[1024,512]{1,0:T(8,128)(2,1)}), bf16[1024,2048]{1,0:T(8,128)(2,1)}) %all-gather.11.cloned.1.call-update) | async-done | bytes 4194320 | tf_op jit(solution)/shard_map/all_gather | solution.py:65
  166.5 7.0 %fusion = bf16[1,512,2048]{2,1,0:T(8,128)(2,1)} fusion(bf16[1024,2048]{1,0:T(8,128)(2,1)} %all-gather.11.cloned.1.call-done, f32[512,1024]{1,0:T(8,128)} %copy-done.1, f32[1024]{0:T(1024)S(1)} %copy-done.5, f32[1024]{0:T(1024)S(1)} %copy-done.6, f32[512]{0:T(512)S(1)} %add_rsqrt_fusion, f32[512]{0:T(512)S(1)} %broadcast_multiply_fusion), kind=kOutput, calls=%fused_computation.1 | convolution fusion | flops 2153250816 | bytes 8400896 | tf_op jit(solution)/shard_map/dot_general | solution.py:63
  (24 shorter events, 0.3 us)
Async XLA Ops:
  6.5 124.1 %copy-start = (bf16[1,512,2048]{2,1,0:T(8,128)(2,1)S(1)}, bf16[1,512,2048]{2,1,0:T(8,128)(2,1)}, u32[]{:S(2)}) copy-start(bf16[1,512,2048]{2,1,0:T(8,128)(2,1)} %param.8) | copy-start | bytes 6291460
  6.5 33.1 %all-gather.5.cloned.1.call-start = ((), (), s32[]{:S(2)}) async-start(), calls=%async_computation | async-start | bytes 1310720 | tf_op jit(solution)/shard_map/all_gather | solution.py:33
  7.3 61.3 %all-gather.7.cloned.1.call-start = ((), (), s32[]{:S(2)}) async-start(), calls=%async_computation.1 | async-start | bytes 1310720 | tf_op jit(solution)/shard_map/all_gather | solution.py:34
  8.0 122.6 %all-gather.9.cloned.1.call-start = ((), (), s32[]{:S(2)}) async-start(), calls=%async_computation.2 | async-start | bytes 10485760 | tf_op jit(solution)/shard_map/all_gather | solution.py:40
  71.7 0.9 copy-start.2
  71.7 94.8 %all-gather.11.cloned.1.call-start = ((), (), s32[]{:S(2)}) async-start(), calls=%async_computation.3 | async-start | bytes 5242880 | tf_op jit(solution)/shard_map/all_gather | solution.py:65
  72.6 9.4 %collective-permute-start.1 = (bf16[256,512]{1,0:T(8,128)(2,1)S(1)}, bf16[256,512]{1,0:T(8,128)(2,1)S(1)}, u32[]{:S(2)}, u32[]{:S(2)}) collective-permute-start(bf16[256,512]{1,0:T(8,128)(2,1)S(1)} %copy-done.2), channel_id=1, source_target_pairs={{0,4},{4,8},{8,12},{12,0},{1,5},{5,9},{9,13},{13,1},{2,6},{6,10},{... | collective-permute-start | bytes 786440 | tf_op jit(solution)/shard_map/ppermute | solution.py:14
  82.0 8.5 %collective-permute-start.2 = (bf16[256,512]{1,0:T(8,128)(2,1)S(1)}, bf16[256,512]{1,0:T(8,128)(2,1)S(1)}, u32[]{:S(2)}, u32[]{:S(2)}) collective-permute-start(bf16[256,512]{1,0:T(8,128)(2,1)S(1)} %collective-permute-done.1), channel_id=1, source_target_pairs={{0,4},{4,8},{8,12},{12,0},{1,5},{5,9},{9,13},{13,1},{2,6},{6,10},{... | collective-permute-start | bytes 786440 | tf_op jit(solution)/shard_map/ppermute | solution.py:14
  90.5 8.2 %collective-permute-start.3 = (bf16[256,512]{1,0:T(8,128)(2,1)S(1)}, bf16[256,512]{1,0:T(8,128)(2,1)S(1)}, u32[]{:S(2)}, u32[]{:S(2)}) collective-permute-start(bf16[256,512]{1,0:T(8,128)(2,1)S(1)} %collective-permute-done.2), channel_id=1, source_target_pairs={{0,4},{4,8},{8,12},{12,0},{1,5},{5,9},{9,13},{13,1},{2,6},{6,10},{... | collective-permute-start | bytes 786440 | tf_op jit(solution)/shard_map/ppermute | solution.py:14
  98.8 1.2 copy-start.3
  139.3 5.3 %collective-permute-start = (bf16[30,1024]{1,0:T(8,128)(2,1)S(1)}, bf16[30,1024]{1,0:T(8,128)(2,1)S(1)}, u32[]{:S(2)}, u32[]{:S(2)}) collective-permute-start(bf16[30,1024]{1,0:T(8,128)(2,1)S(1)} %slice_bitcast_fusion), channel_id=1, source_target_pairs={{0,4},{4,8},{8,12},{1,5},{5,9},{9,13},{2,6},{6,10},{10,14},{3,7},{... | collective-permute-start | bytes 184328 | tf_op jit(solution)/shard_map/ppermute | solution.py:23
  143.3 1.6 copy-start.4
  154.7 1.3 copy-start.1
  154.8 11.7 %copy-start.5 = (f32[1024]{0:T(1024)S(1)}, f32[1024]{0:T(1024)}, u32[]{:S(2)}) copy-start(f32[1024]{0:T(1024)} %param.14) | copy-start | bytes 12292
  154.8 11.7 %copy-start.6 = (f32[1024]{0:T(1024)S(1)}, f32[1024]{0:T(1024)}, u32[]{:S(2)}) copy-start(f32[1024]{0:T(1024)} %param.13) | copy-start | bytes 12292
Sparse Core Ops, SparseCore 0:
  8.9 30.6 all-gather.4
  41.2 27.3 all-gather.6
  71.8 58.7 all-gather.8
  132.0 34.4 all-gather.10
